TPU v7x, 32 devices: a whole 2x2x4 slice. The times are simulated.
32 devices in a mesh: kv: 8 (over z, x), tp: 4 (over y, core).
Axes of the slice: x: 2, y: 2, z: 4, core: 2. Of those that a mesh axis runs over, the one named last changes fastest.
Arguments:
- tokens: bfloat16 [256, 2048], P('kv', 'tp'), may hold values from -60 to 60, as said below
- memory: float32 [256, 8, 128, 128], P('kv', 'tp'), may hold values from -0.6 to 0.6
- normalizer: float32 [256, 8, 128], P('kv', 'tp'), may hold values from -0.6 to 0.6
- stabilizer: float32 [256, 8], P('kv', 'tp'), may hold values from -4 to 4
- norm_gain: float32 [2048], replicated, may hold values from 0.1 to 1.9
- query_weight: bfloat16 [2048, 1024], P(None, 'tp'), may hold values from -0.125 to 0.125
- key_weight: bfloat16 [2048, 1024], P(None, 'tp'), may hold values from -0.125 to 0.125
- value_weight: bfloat16 [2048, 1024], P(None, 'tp'), may hold values from -0.125 to 0.125
- outgate_weight: bfloat16 [2048, 1024], P(None, 'tp'), may hold values from -0.125 to 0.125
- input_gate_weight: bfloat16 [2048, 8], replicated, may hold values from -0.125 to 0.125
- forget_gate_weight: bfloat16 [2048, 8], replicated, may hold values from -0.125 to 0.125
- forget_bias: float32 [8], replicated, may hold values from -1 to 5
- memory_gain: float32 [1024], P('tp'), may hold values from 0.1 to 1.9
- proj_weight: bfloat16 [1024, 2048], P(None, 'tp'), may hold values from -0.1875 to 0.1875
- ffn_gain: float32 [2048], P('tp'), may hold values from 0.1 to 1.9
- up_weight: bfloat16 [2048, 8192], P('tp', 'kv'), may hold values from -0.125 to 0.125
- down_weight: bfloat16 [8192, 2048], P('kv', 'tp'), may hold values from -0.0625 to 0.0625
Outputs:
- layer_out: bfloat16 [256, 2048], P('kv', 'tp')
- memory_new: float32 [256, 8, 128, 128], P('kv', 'tp')
- normalizer_new: float32 [256, 8, 128], P('kv', 'tp')
- stabilizer_new: float32 [256, 8], P('kv', 'tp')
Inputs may be any that keep to these rules, and one draw needn't show every extreme that they name: `tokens`: activations whose feature blocks and rows differ in scale.
All inputs are finite; a program needn't handle non-finite values.
Results may differ from a plain program's by a relative error of at most 0.0095.
Values may be sent and summed in bfloat16 or wider, within the bound.
A program may use at most 64 MiB of HBM per device.

v0:
```python
import jax
import jax.numpy as jnp
from jax import lax
from jax.sharding import PartitionSpec as P

D = 2048
DK = 128
DV = 128


EPS = 1e-06


def per_device(
    tokens,
    memory,
    normalizer,
    stabilizer,
    norm_gain,
    query_weight,
    key_weight,
    value_weight,
    outgate_weight,
    input_gate_weight,
    forget_gate_weight,
    forget_bias,
    memory_gain,
    proj_weight,
    ffn_gain,
    up_weight,
    down_weight,
):
    own_rows = tokens.shape[0]
    heads_here = memory.shape[1]
    first_head = lax.axis_index("tp") * heads_here
    full_rows = lax.all_gather(tokens, "tp", axis=1, tiled=True)
    rows_f = full_rows.astype(jnp.float32)
    scale_one = lax.rsqrt(jnp.mean(rows_f * rows_f, axis=-1, keepdims=True) + EPS)
    normed = (rows_f * scale_one * norm_gain).astype(jnp.bfloat16)
    query = jnp.dot(normed, query_weight, preferred_element_type=jnp.float32).astype(jnp.bfloat16)
    keys = jnp.dot(normed, key_weight, preferred_element_type=jnp.float32).astype(jnp.bfloat16)
    values = jnp.dot(normed, value_weight, preferred_element_type=jnp.float32).astype(jnp.bfloat16)
    gate_out = jnp.dot(normed, outgate_weight, preferred_element_type=jnp.float32).astype(
        jnp.bfloat16
    )
    input_cols = lax.dynamic_slice_in_dim(input_gate_weight, first_head, heads_here, 1)
    forget_cols = lax.dynamic_slice_in_dim(forget_gate_weight, first_head, heads_here, 1)
    bias_here = lax.dynamic_slice_in_dim(forget_bias, first_head, heads_here, 0)
    input_log = jnp.dot(normed, input_cols, preferred_element_type=jnp.float32)
    forget_log = jax.nn.log_sigmoid(
        jnp.dot(normed, forget_cols, preferred_element_type=jnp.float32) + bias_here
    )
    query_f = query.astype(jnp.float32).reshape(own_rows, heads_here, DK)
    keys_f = keys.astype(jnp.float32).reshape(own_rows, heads_here, DK) * DK ** (-0.5)
    values_f = values.astype(jnp.float32).reshape(own_rows, heads_here, DV)
    stab_new = jnp.maximum(forget_log + stabilizer, input_log)
    keep = jnp.exp(forget_log + stabilizer - stab_new)
    admit = jnp.exp(input_log - stab_new)
    memory_new = (
        keep[..., None, None] * memory
        + admit[..., None, None] * values_f[..., :, None] * keys_f[..., None, :]
    )
    normalizer_new = keep[..., None] * normalizer + admit[..., None] * keys_f
    numer = jnp.einsum("bhed,bhd->bhe", memory_new, query_f, precision=lax.Precision.HIGHEST)
    denom = jnp.sum(normalizer_new * query_f, axis=-1)
    cell = numer / jnp.maximum(jnp.abs(denom), 1.0)[..., None]
    mixed = (
        cell.reshape(own_rows, heads_here * DV)
        * memory_gain
        * jax.nn.sigmoid(gate_out.astype(jnp.float32))
    ).astype(jnp.bfloat16)
    projected = jnp.dot(
        lax.all_gather(mixed, "tp", axis=1, tiled=True),
        proj_weight,
        preferred_element_type=jnp.float32,
    )
    second = (tokens.astype(jnp.float32) + projected).astype(jnp.bfloat16)
    all_rows = lax.all_gather(second, "kv", axis=0, tiled=True)
    all_f = all_rows.astype(jnp.float32)
    square_sum = jnp.sum(all_f * all_f, axis=-1)
    scaled = (all_f * ffn_gain).astype(jnp.bfloat16)
    preact = jnp.dot(scaled, up_weight, preferred_element_type=jnp.float32)
    share = lax.psum_scatter(preact, "tp", scatter_dimension=1, tiled=True)
    square_sum = lax.psum(square_sum, "tp")
    scale_two = lax.rsqrt(square_sum / D + EPS)
    partial_hidden = jnp.square(jax.nn.relu(share * scale_two[:, None])).astype(jnp.bfloat16)
    hidden = lax.all_gather(partial_hidden, "tp", axis=1, tiled=True)
    summed = lax.psum_scatter(
        jnp.dot(hidden, down_weight, preferred_element_type=jnp.float32),
        "kv",
        scatter_dimension=0,
        tiled=True,
    )
    layer_out = (second.astype(jnp.float32) + summed).astype(jnp.bfloat16)
    return (layer_out, memory_new, normalizer_new, stab_new)


def solution(mesh):
    placed = (
        P("kv", "tp"),
        P("kv", "tp", None, None),
        P("kv", "tp", None),
        P("kv", "tp"),
        P(),
        P(None, "tp"),
        P(None, "tp"),
        P(None, "tp"),
        P(None, "tp"),
        P(),
        P(),
        P(),
        P("tp"),
        P(None, "tp"),
        P("tp"),
        P("tp", "kv"),
        P("kv", "tp"),
    )
    return jax.shard_map(
        per_device,
        mesh=mesh,
        in_specs=placed,
        out_specs=(P("kv", "tp"), P("kv", "tp", None, None), P("kv", "tp", None), P("kv", "tp")),
        check_vma=False,
    )
```

profile of v0, /device:TPU:0, one launch (start us, length us, event | category | flops | bytes accessed | tf_op | source)
XLA Modules:
  0.0 177.4 jit_solution(6909236550511588399)
XLA Ops:
  7.2 0.0 copy-start
  7.2 0.0 copy-start.7
  7.2 0.0 reduce-scatter.3.cloned.1.call-start
  7.2 6.9 %all_gather.12 = bf16[32,2048]{1,0:T(8,128)(2,1)S(1)} all-gather(bf16[32,512]{1,0:T(8,128)(2,1)} %param.17), channel_id=1, replica_groups=mesh['kv'=8,'tp'=4] {'tp'}, dimensions={1}, use_global_device_ids=true | all-gather | bytes 163840 | tf_op jit(solution)/shard_map/all_gather | solution.py:36
  14.1 0.1 fusion.13
  14.3 1.6 convolution_convert_fusion.1
  15.9 0.7 dynamic_slice.10
  16.6 1.0 fusion.23
  17.6 1.0 broadcast_multiply_fusion.2
  18.6 0.1 copy.21
  18.7 0.1 copy.24
  18.8 0.1 copy.22
  18.9 1.6 fusion.9
  20.5 1.6 fusion.8
  22.1 0.0 copy-done.7
  22.1 0.8 multiply_reduce_fusion
  22.9 3.7 %multiply_add_fusion = f32[32,2,128,128]{3,2,1,0:T(8,128)S(1)} fusion(f32[32,2,128,128]{3,2,1,0:T(8,128)} %param.18, f32[32,2,128]{2,1,0:T(2,128)S(1)} %get-tuple-element.9, f32[32,2,128]{2,1,0:T(2,128)S(1)} %get-tuple-element.10, f32[32,2]{1,0:T(8,128)S(1)} %copy.21), kind=kLoop, calls=%fused_computation | loop fusion | flops 3145728 | bytes 8454400 | tf_op jit(solution)/shard_map/add | solution.py:60
  26.6 0.0 copy-done.9
  26.6 0.0 copy-start.1
  26.6 2.0 %copy-done.1 = f32[32,2,128,128]{3,2,1,0:T(8,128)} copy-done((f32[32,2,128,128]{3,2,1,0:T(8,128)}, f32[32,2,128,128]{3,2,1,0:T(8,128)S(1)}, u32[]{:S(2)}) %copy-start.1) | copy-done | bytes 4194328
  28.6 0.0 copy-start.6
  28.6 0.0 copy-start.8
  28.6 3.3 %fusion.34 = f32[32,2,1,128]{3,2,1,0:T(1,128)S(1)} fusion(f32[32,2,128,128]{3,2,1,0:T(8,128)S(1)} %multiply_add_fusion, bf16[32,2,128,1]{2,3,1,0:T(2,128)(2,1)S(1)} %reshape.70), kind=kOutput, calls=%fused_computation.51 | convolution fusion | flops 12582912 | bytes 4243456 | tf_op jit(solution)/shard_map/bhed,bhd->bhe/dot_general | solution.py:64
  32.0 0.1 broadcast_divide_fusion
  32.1 0.0 copy-done.3
  32.1 0.0 copy-done.5
  32.1 0.0 copy-done.10
  32.2 0.3 fusion.7
  32.5 5.4 %all_gather.13 = bf16[32,1024]{1,0:T(8,128)(2,1)S(1)} all-gather(bf16[32,256]{1,0:T(8,128)(2,1)S(1)} %fusion.7), channel_id=1, replica_groups=mesh['kv'=8,'tp'=4] {'tp'}, dimensions={1}, use_global_device_ids=true | all-gather | bytes 81920 | tf_op jit(solution)/shard_map/all_gather | solution.py:73
  37.9 0.0 copy-done.2
  37.9 0.0 copy-done.6
  37.9 0.3 fusion
  38.2 31.4 %all_gather.14 = bf16[256,512]{1,0:T(8,128)(2,1)S(1)} all-gather(bf16[32,512]{1,0:T(8,128)(2,1)S(1)} %fusion), channel_id=1, replica_groups=mesh['kv'=8,'tp'=4] {'kv'}, dimensions={0}, use_global_device_ids=true | all-gather | bytes 294912 | tf_op jit(solution)/shard_map/all_gather | solution.py:78
  69.6 0.0 copy-done
  69.6 0.0 copy-done.8
  69.6 1.4 fusion.16
  71.0 0.0 reduce-scatter.3.cloned.1.call-update
  71.0 0.0 reduce-scatter.5.cloned.1.call-start
  71.1 0.1 fusion.12
  71.2 5.7 %psum.7 = f32[256]{0:T(256)S(1)} all-reduce(f32[256]{0:T(256)S(1)} %fusion.12), channel_id=1, replica_groups=mesh['kv'=8,'tp'=4] {'tp'}, use_global_device_ids=true, to_apply=%region_4.5 | all-reduce | flops 256 | bytes 2048 | tf_op jit(solution)/shard_map/psum | solution.py:84
  76.9 19.9 %reduce-scatter.3.cloned.1.call-done = f32[256,256]{1,0:T(8,128)} async-done(((f32[256,1024]{1,0:T(8,128)}), f32[256,256]{1,0:T(8,128)}) %reduce-scatter.3.cloned.1.call-update) | async-done | bytes 262160 | tf_op jit(solution)/shard_map/reduce_scatter | solution.py:83
  96.8 1.1 multiply_convert_fusion
  97.8 6.6 %all_gather.15 = bf16[256,1024]{1,0:T(8,128)(2,1)S(1)} all-gather(bf16[256,256]{1,0:T(8,128)(2,1)S(1)} %multiply_convert_fusion), channel_id=1, replica_groups=mesh['kv'=8,'tp'=4] {'tp'}, dimensions={1}, use_global_device_ids=true | all-gather | bytes 655360 | tf_op jit(solution)/shard_map/all_gather | solution.py:87
  104.4 0.0 copy-done.4
  104.4 1.2 fusion.35
  105.7 0.0 reduce-scatter.5.cloned.1.call-update
  105.7 63.4 %reduce-scatter.5.cloned.1.call-done = f32[32,512]{1,0:T(8,128)} async-done(((f32[256,512]{1,0:T(8,128)}), f32[32,512]{1,0:T(8,128)}) %reduce-scatter.5.cloned.1.call-update) | async-done | bytes 65552 | tf_op jit(solution)/shard_map/reduce_scatter | solution.py:88
  169.1 1.5 add_convert_fusion
  (14 shorter events, 0.1 us)
Async XLA Ops:
  7.2 62.4 %copy-start = (bf16[512,1024]{1,0:T(8,128)(2,1)S(1)}, bf16[512,1024]{1,0:T(8,128)(2,1)}, u32[]{:S(2)}) copy-start(bf16[512,1024]{1,0:T(8,128)(2,1)} %param.32) | copy-start | bytes 3145732
  7.2 14.9 %copy-start.7 = (f32[32,2,128]{2,1,0:T(2,128)S(1)}, f32[32,2,128]{2,1,0:T(2,128)}, u32[]{:S(2)}) copy-start(f32[32,2,128]{2,1,0:T(2,128)} %param.19) | copy-start | bytes 98308
  7.2 89.6 %reduce-scatter.3.cloned.1.call-start = ((), (), s32[]{:S(2)}) async-start(), calls=%async_computation.2 | async-start | bytes 1310720 | tf_op jit(solution)/shard_map/reduce_scatter | solution.py:83
  18.6 8.0 %copy-start.9 = (f32[32,2]{0,1:T(2,128)}, f32[32,2]{0,1:T(2,128)S(1)}, u32[]{:S(2)}) copy-start(f32[32,2]{0,1:T(2,128)S(1)} %get-tuple-element.8) | copy-start | bytes 772
  26.6 2.0 %copy-start.1 = (f32[32,2,128,128]{3,2,1,0:T(8,128)}, f32[32,2,128,128]{3,2,1,0:T(8,128)S(1)}, u32[]{:S(2)}) copy-start(f32[32,2,128,128]{3,2,1,0:T(8,128)S(1)} %multiply_add_fusion) | copy-start | bytes 12582916
  28.6 3.5 %copy-start.3 = (bf16[2048,256]{1,0:T(8,128)(2,1)S(1)}, bf16[2048,256]{1,0:T(8,128)(2,1)}, u32[]{:S(2)}) copy-start(bf16[2048,256]{1,0:T(8,128)(2,1)} %param.25) | copy-start | bytes 3145732
  28.6 3.5 %copy-start.5 = (f32[2048]{0:T(1024)S(1)}, f32[2048]{0:T(1024)}, u32[]{:S(2)}) copy-start(f32[2048]{0:T(1024)} %param.21) | copy-start | bytes 24580
  28.6 3.5 %copy-start.10 = (f32[256]{0:T(256)S(1)}, f32[256]{0:T(256)}, u32[]{:S(2)}) copy-start(f32[256]{0:T(256)} %param.29) | copy-start | bytes 3076
  28.6 9.3 %copy-start.2 = (bf16[1024,512]{1,0:T(8,128)(2,1)S(1)}, bf16[1024,512]{1,0:T(8,128)(2,1)}, u32[]{:S(2)}) copy-start(bf16[1024,512]{1,0:T(8,128)(2,1)} %param.30) | copy-start | bytes 3145732
  28.6 9.3 %copy-start.6 = (bf16[32,512]{1,0:T(8,128)(2,1)S(1)}, bf16[32,512]{1,0:T(8,128)(2,1)}, u32[]{:S(2)}) copy-start(bf16[32,512]{1,0:T(8,128)(2,1)} %param.17) | copy-start | bytes 98308
  28.6 40.9 %copy-start.8 = (f32[512]{0:T(512)S(1)}, f32[512]{0:T(512)}, u32[]{:S(2)}) copy-start(f32[512]{0:T(512)} %param.31) | copy-start | bytes 6148
  32.0 72.4 %copy-start.4 = (bf16[1024,512]{1,0:T(8,128)(2,1)S(1)}, bf16[1024,512]{1,0:T(8,128)(2,1)}, u32[]{:S(2)}) copy-start(bf16[1024,512]{1,0:T(8,128)(2,1)} %param.33) | copy-start | bytes 3145732
  71.0 98.1 %reduce-scatter.5.cloned.1.call-start = ((), (), s32[]{:S(2)}) async-start(), calls=%async_computation.3 | async-start | bytes 589824 | tf_op jit(solution)/shard_map/reduce_scatter | solution.py:88
Sparse Core Ops, SparseCore 0:
  71.1 25.5 reduce-scatter.2
  105.8 63.2 reduce-scatter.4
where the time goes:
time: 178 us; the launch traced here: 177 us
  waiting for transfers between devices  83.3 us (47%)
  blocking collectives  55.9 us (31%)
  between operations  14.2 us (8%)
  matrix products  13.3 us (7%)
  other arithmetic  7.4 us (4%)
  local copies, waits for them, and re-layouts  3.12 us (2%)
    reduce_scatter x1, waiting for transfers between devices, per_device(): lax.psum_scatter(jnp.dot(hidden, down_weight, preferred_element_type=jnp....  63.4 us
    all_gather x1, blocking collectives, per_device(): all_rows = lax.all_gather(second, 'kv', axis=0, tiled=True)  31.4 us
    reduce_scatter x1, waiting for transfers between devices, per_device(): share = lax.psum_scatter(preact, 'tp', scatter_dimension=1, tiled=True)  19.9 us
    all_gather x1, blocking collectives, per_device(): full_rows = lax.all_gather(tokens, 'tp', axis=1, tiled=True)  6.88 us
    all_gather x1, blocking collectives, per_device(): hidden = lax.all_gather(partial_hidden, 'tp', axis=1, tiled=True)  6.61 us
    psum x1, blocking collectives, per_device(): square_sum = lax.psum(square_sum, 'tp')  5.67 us
    all_gather x1, blocking collectives, per_device(): lax.all_gather(mixed, 'tp', axis=1, tiled=True)  5.41 us
    add x1, other arithmetic, per_device(): keep[..., None, None] * memory  3.69 us
  transfers between devices with their start and end apart: 2, of which 2 were waited for; matrix products, arithmetic and copies ran while one was open for 0% of the time, Pallas kernels for 0%

commit v1 on v0

v1 whole, which is shorter than its diff:
```python
import functools

import jax
import jax.numpy as jnp
from jax import lax
from jax.experimental import pallas as pl
from jax.experimental.pallas import tpu as pltpu
from jax.sharding import PartitionSpec as P

EPS = 1e-06
LANES = 128
GROUP = 16
LAG2, LAG3, LAG4 = 1, 2, 3
F32, BF16 = jnp.float32, jnp.bfloat16


def dot(a, b):
    return jnp.dot(a, b, preferred_element_type=F32)


def layer_kernel(
    nkv,
    ntp,
    tok,
    mem_h,
    nrm,
    stab,
    ngain,
    wq_h,
    wk_h,
    wv_h,
    wo_h,
    wig,
    wfg,
    fbias,
    mgain,
    wp_h,
    fgain,
    wu_h,
    wd_h,
    out,
    nrm_new,
    stab_new,
    keep_out,
    av_out,
    key_out,
    mem,
    wqkv,
    wp,
    wu,
    wd,
    tokg,
    mixg,
    secg,
    pown,
    xa_s,
    xa_r,
    yb_s,
    yb_r,
    hid,
    hid_r,
    sq_s,
    sq_r,
    part_s,
    part_r,
    down_own,
    w_sem,
    p_sem,
    f_sem,
    m_sem,
    tp_send,
    tp_recv,
    mx_send,
    mx_recv,
    kv_send,
    kv_recv,
    a_send,
    a_recv,
    b_send,
    b_recv,
    c_send,
    c_recv,
    q_send,
    q_recv,
    r_send,
    r_recv,
):
    rows, width = tok.shape
    heads, dk = nrm.shape[1], nrm.shape[2]
    cols = heads * dk
    features = width * ntp
    half = wu.shape[2]
    ny, nz = ntp // 2, nkv // 2
    me_tp, me_kv = lax.axis_index("tp"), lax.axis_index("kv")
    y, core = me_tp // 2, me_tp % 2
    z, x = me_kv // 2, me_kv % 2
    tps = [(dy, dc) for dy in range(ny) for dc in range(2)]
    kvs = [(dz, dx) for dz in range(nz) for dx in range(2)]

    def tp_at(dy, dc):
        return ((y + dy + ny) % ny) * 2 + (core + dc + 2) % 2

    def kv_at(dz, dx):
        return ((z + dz + nz) % nz) * 2 + (x + dx + 2) % 2

    wcopies = []
    for d, (dy, dc) in enumerate(tps):
        src = tp_at(-dy, -dc)
        group = []
        for j, w in enumerate((wq_h, wk_h, wv_h, wo_h)):
            cp = pltpu.make_async_copy(
                w.at[pl.ds(pl.multiple_of(src * width, width), width), :],
                wqkv.at[d, :, pl.ds(j * cols, cols)],
                w_sem.at[d, j],
            )
            cp.start()
            group.append(cp)
        wcopies.append(group)
    mcopy = pltpu.make_async_copy(mem_h, mem, m_sem.at[0])
    mcopy.start()
    pcopies = []
    for d, (dy, dc) in enumerate(tps):
        src = tp_at(-dy, -dc)
        cp = pltpu.make_async_copy(
            wp_h.at[pl.ds(pl.multiple_of(src * cols, cols), cols), :], wp.at[d], p_sem.at[d]
        )
        cp.start()
        pcopies.append(cp)
    fcopies = []
    for i in range(2):
        at = pl.ds(pl.multiple_of(((core + i) % 2) * half, half), half)
        for j, (s, t) in enumerate(((wu_h.at[:, at], wu.at[i]), (wd_h.at[at, :], wd.at[i]))):
            cp = pltpu.make_async_copy(s, t, f_sem.at[i, j])
            cp.start()
            fcopies.append(cp)

    barrier = pltpu.get_barrier_semaphore()
    for dy, dc in tps[1:]:
        pl.semaphore_signal(
            barrier, inc=1, device_id={"tp": tp_at(dy, dc)}, device_id_type=pl.DeviceIdType.MESH
        )
    for dz, dx in kvs[1:]:
        pl.semaphore_signal(
            barrier, inc=1, device_id={"kv": kv_at(dz, dx)}, device_id_type=pl.DeviceIdType.MESH
        )
    pl.semaphore_wait(barrier, ntp + nkv - 2)

    sends = []

    def send(src, dst, s_sem, r_sem, device):
        cp = pltpu.make_async_remote_copy(
            src_ref=src,
            dst_ref=dst,
            send_sem=s_sem,
            recv_sem=r_sem,
            device_id=device,
            device_id_type=pl.DeviceIdType.MESH,
        )
        cp.start()
        sends.append(cp)
        return cp

    tok_in = [None]
    for d, (dy, dc) in enumerate(tps):
        if d:
            tok_in.append(
                send(tok, tokg.at[d], tp_send.at[d], tp_recv.at[d], {"tp": tp_at(dy, dc)})
            )
    acc = jnp.zeros((rows, 4 * cols), F32)
    in_acc = jnp.zeros((rows, wig.shape[1]), F32)
    fg_acc = jnp.zeros((rows, wig.shape[1]), F32)
    square = jnp.zeros((rows, 1), F32)
    for d, (dy, dc) in enumerate(tps):
        src = tp_at(-dy, -dc)
        at = pl.ds(pl.multiple_of(src * width, width), width)
        if d:
            tok_in[d].wait_recv()
        block = (tokg[d] if d else tok[...]).astype(F32)
        square += jnp.sum(block * block, axis=1, keepdims=True)
        gained = (block * ngain[:, at]).astype(BF16)
        for cp in wcopies[d]:
            cp.wait()
        acc += dot(gained, wqkv[d])
        in_acc += dot(gained, wig[at, :])
        fg_acc += dot(gained, wfg[at, :])
    scale = lax.rsqrt(square / features + EPS)
    acc = acc * scale
    lane = lax.broadcasted_iota(jnp.int32, in_acc.shape, 1)
    in_acc = in_acc * scale
    fg_acc = jax.nn.log_sigmoid(fg_acc * scale + fbias[...])

    mcopy.wait()
    pick = lax.broadcasted_iota(jnp.int32, (GROUP, dk), 0)
    for h in range(heads):
        mine = lane == me_tp * heads + h
        input_log = jnp.sum(jnp.where(mine, in_acc, 0.0), axis=1, keepdims=True)
        forget_log = jnp.sum(jnp.where(mine, fg_acc, 0.0), axis=1, keepdims=True)
        query, keys, values, gate = (
            acc[:, j * cols + h * dk : j * cols + (h + 1) * dk].astype(BF16) for j in range(4)
        )
        query_f, values_f, gate_f = query.astype(F32), values.astype(F32), gate.astype(F32)
        keys_f = keys.astype(F32) * dk**-0.5
        carried = forget_log + stab[:, h : h + 1]
        newest = jnp.maximum(carried, input_log)
        keep = jnp.exp(carried - newest)
        admit = jnp.exp(input_log - newest)
        norm_h = keep * nrm[:, h, :] + admit * keys_f
        nrm_new[:, h, :] = norm_h
        stab_new[:, h : h + 1] = newest
        keep_out[:, h : h + 1] = keep
        av_out[:, h, :] = admit * values_f
        key_out[:, h, :] = keys_f
        read = []
        for g in range(rows // GROUP):
            m = mem[g * GROUP : (g + 1) * GROUP, h].reshape(GROUP * dk, dk).astype(BF16)
            r = lax.dot_general(
                query[g * GROUP : (g + 1) * GROUP],
                m,
                (((1,), (1,)), ((), ())),
                preferred_element_type=F32,
            )
            total = jnp.zeros((GROUP, dk), F32)
            for i in range(GROUP):
                total = jnp.where(pick == i, r[:, i * dk : (i + 1) * dk], total)
            read.append(total)
        held = jnp.concatenate(read, axis=0)
        numer = keep * held + (
            admit * jnp.sum(keys_f * query_f, axis=1, keepdims=True)
        ) * values_f
        denom = jnp.sum(norm_h * query_f, axis=1, keepdims=True)
        cell = numer / jnp.maximum(jnp.abs(denom), 1.0)
        mixed = cell * mgain[:, h * dk : (h + 1) * dk] * jax.nn.sigmoid(gate_f)
        mixg[0, :, h * dk : (h + 1) * dk] = mixed.astype(BF16)

    mix_in = [None]
    for d, (dy, dc) in enumerate(tps):
        if d:
            mix_in.append(
                send(mixg.at[0], mixg.at[d], mx_send.at[d], mx_recv.at[d], {"tp": tp_at(dy, dc)})
            )
    second = tok[...].astype(F32)
    for d in range(ntp):
        if d:
            mix_in[d].wait_recv()
        pcopies[d].wait()
        second += dot(mixg[d], wp[d])
    secg[0, 0] = second.astype(BF16)

    sec_in = {}
    for dz, dx in kvs[1:]:
        sec_in[dz, dx] = send(
            secg.at[0, 0],
            secg.at[dz, dx],
            kv_send.at[dz, dx],
            kv_recv.at[dz, dx],
            {"kv": kv_at(dz, dx)},
        )
    for cp in fcopies:
        cp.wait()

    a_in, b_in, c_in, q_in, r_in = {}, {}, {}, {}, {}
    other_core = {"tp": tp_at(0, 1)}

    def stage1(c):
        for dx in range(2):
            if (c, dx) != (0, 0):
                sec_in[c, dx].wait_recv()
        block = secg[c].reshape(2 * rows, width).astype(F32)
        scaled = (block * fgain[...]).astype(BF16)
        xa_s[c] = dot(scaled, wu[1]).astype(BF16)
        a_in[c] = send(xa_s.at[c], xa_r.at[c], a_send.at[c], a_recv.at[c], other_core)
        squares = jnp.sum(block * block, axis=1, keepdims=True)
        wide = jnp.concatenate(
            [
                jnp.broadcast_to(squares, (2 * rows, LANES)),
                jnp.zeros((LANES - 2 * rows, LANES), F32),
            ],
            axis=0,
        )
        sq_s[c] = jnp.transpose(wide)[:8]
        q_in[c] = [
            send(
                sq_s.at[c],
                sq_r.at[c, d - 1],
                q_send.at[c, d - 1],
                q_recv.at[c, d - 1],
                {"tp": tp_at(*tps[d])},
            )
            for d in range(1, ntp)
        ]
        pown[c] = dot(scaled, wu[0])

    def stage2(c):
        a_in[c].wait_recv()
        both = pown[c] + xa_r[c].astype(F32)
        pown[c] = both
        yb_s[c] = both.astype(BF16)
        b_in[c] = [
            send(
                yb_s.at[c],
                yb_r.at[c, d - 1],
                b_send.at[c, d - 1],
                b_recv.at[c, d - 1],
                {"tp": tp_at(d, 0)},
            )
            for d in range(1, ny)
        ]

    def stage3(c):
        total = sq_s[c]
        for d in range(ntp - 1):
            q_in[c][d].wait_recv()
            total = total + sq_r[c, d]
        tall = jnp.transpose(jnp.broadcast_to(total[0:1], (LANES, LANES)))
        scale_two = lax.rsqrt(tall[: 2 * rows, 0:1] / features + EPS)
        summed = pown[c]
        for d in range(ny - 1):
            b_in[c][d].wait_recv()
            summed = summed + yb_r[c, d].astype(F32)
        hid[c] = jnp.square(jnp.maximum(summed * scale_two, 0.0)).astype(BF16)
        c_in[c] = send(hid.at[c], hid_r.at[c], c_send.at[c], c_recv.at[c], other_core)

    def stage4(c):
        part = dot(hid[c], wd[0])
        c_in[c].wait_recv()
        part = part + dot(hid_r[c], wd[1])
        for dx in range(2):
            piece = part[dx * rows : (dx + 1) * rows]
            if (c, dx) == (0, 0):
                down_own[...] = piece
                continue
            part_s[c, dx] = piece.astype(BF16)
            r_in[c, dx] = send(
                part_s.at[c, dx],
                part_r.at[c, dx],
                r_send.at[c, dx],
                r_recv.at[c, dx],
                {"kv": kv_at(-c, dx)},
            )

    for t in range(nz + LAG4):
        for lag, stage in ((0, stage1), (LAG2, stage2), (LAG3, stage3), (LAG4, stage4)):
            if 0 <= t - lag < nz:
                stage(t - lag)

    result = secg[0, 0].astype(F32) + down_own[...]
    for dz, dx in kvs[1:]:
        r_in[dz, dx].wait_recv()
        result += part_r[dz, dx].astype(F32)
    out[...] = result.astype(BF16)
    for cp in sends:
        cp.wait_send()


def per_device(
    nkv,
    ntp,
    tokens,
    memory,
    normalizer,
    stabilizer,
    norm_gain,
    query_weight,
    key_weight,
    value_weight,
    outgate_weight,
    input_gate_weight,
    forget_gate_weight,
    forget_bias,
    memory_gain,
    proj_weight,
    ffn_gain,
    up_weight,
    down_weight,
):
    rows, width = tokens.shape
    heads, dk = normalizer.shape[1:]
    cols = heads * dk
    half = up_weight.shape[1] // 2
    ny, nz = ntp // 2, nkv // 2
    shape = jax.ShapeDtypeStruct
    vmem = pl.BlockSpec(memory_space=pltpu.VMEM)
    hbm = pl.BlockSpec(memory_space=pl.ANY)
    dma = pltpu.SemaphoreType.DMA
    chunk = (nz, 2 * rows, half)
    blocks = (nz, 2, rows, width)
    out, nrm_new, stab_new, keep, av, keys = pl.pallas_call(
        functools.partial(layer_kernel, nkv, ntp),
        out_shape=(
            shape((rows, width), BF16),
            shape((rows, heads, dk), F32),
            shape((rows, heads), F32),
            shape((rows, heads), F32),
            shape((rows, heads, dk), F32),
            shape((rows, heads, dk), F32),
        ),
        in_specs=[
            vmem, hbm, vmem, vmem, vmem, hbm, hbm, hbm, hbm, vmem, vmem, vmem, vmem, hbm, vmem,
            hbm, hbm,
        ],
        out_specs=(vmem,) * 6,
        scratch_shapes=[
            pltpu.VMEM(memory.shape, F32),
            pltpu.VMEM((ntp, width, 4 * cols), BF16),
            pltpu.VMEM((ntp, cols, width), BF16),
            pltpu.VMEM((2, width, half), BF16),
            pltpu.VMEM((2, half, width), BF16),
            pltpu.VMEM((ntp, rows, width), BF16),
            pltpu.VMEM((ntp, rows, cols), BF16),
            pltpu.VMEM(blocks, BF16),
            pltpu.VMEM(chunk, F32),
            pltpu.VMEM(chunk, BF16),
            pltpu.VMEM(chunk, BF16),
            pltpu.VMEM(chunk, BF16),
            pltpu.VMEM((nz, ny - 1, 2 * rows, half), BF16),
            pltpu.VMEM(chunk, BF16),
            pltpu.VMEM(chunk, BF16),
            pltpu.VMEM((nz, 8, LANES), F32),
            pltpu.VMEM((nz, ntp - 1, 8, LANES), F32),
            pltpu.VMEM(blocks, BF16),
            pltpu.VMEM(blocks, BF16),
            pltpu.VMEM((rows, width), F32),
            dma((ntp, 4)),
            dma((ntp,)),
            dma((2, 2)),
            dma((1,)),
            dma((ntp,)),
            dma((ntp,)),
            dma((ntp,)),
            dma((ntp,)),
            dma((nz, 2)),
            dma((nz, 2)),
            dma((nz,)),
            dma((nz,)),
            dma((nz, ny - 1)),
            dma((nz, ny - 1)),
            dma((nz,)),
            dma((nz,)),
            dma((nz, ntp - 1)),
            dma((nz, ntp - 1)),
            dma((nz, 2)),
            dma((nz, 2)),
        ],
        compiler_params=pltpu.CompilerParams(collective_id=0, has_side_effects=True),
        name="layer",
    )(
        tokens,
        memory,
        normalizer,
        stabilizer,
        norm_gain[None, :],
        query_weight,
        key_weight,
        value_weight,
        outgate_weight,
        input_gate_weight,
        forget_gate_weight,
        forget_bias[None, :],
        memory_gain[None, :],
        proj_weight,
        ffn_gain[None, :],
        up_weight,
        down_weight,
    )
    memory_new = keep[..., None, None] * memory + av[..., :, None] * keys[..., None, :]
    return (out, memory_new, nrm_new, stab_new)


def solution(mesh):
    placed = (
        P("kv", "tp"),
        P("kv", "tp", None, None),
        P("kv", "tp", None),
        P("kv", "tp"),
        P(),
        P(None, "tp"),
        P(None, "tp"),
        P(None, "tp"),
        P(None, "tp"),
        P(),
        P(),
        P(),
        P("tp"),
        P(None, "tp"),
        P("tp"),
        P("tp", "kv"),
        P("kv", "tp"),
    )
    return jax.shard_map(
        functools.partial(per_device, mesh.shape["kv"], mesh.shape["tp"]),
        mesh=mesh,
        in_specs=placed,
        out_specs=(P("kv", "tp"), P("kv", "tp", None, None), P("kv", "tp", None), P("kv", "tp")),
        check_vma=False,
    )
```

time: 178 us -> 51.6 us (0.29)
  waiting for transfers between devices: 83.3 us -> 0 us
  blocking collectives: 55.9 us -> 0 us
  Pallas kernels: 0 us -> 38.8 us
  between operations: 14.2 us -> 0.64 us
  matrix products: 13.3 us -> 0 us
  local copies, waits for them, and re-layouts: 3.12 us -> 7.47 us
  other arithmetic: 7.4 us -> 4.36 us
    reduce_scatter x2 -> x0, waiting for transfers between devices: 83.3 us -> none  [the longest x1 63.4 us: per_device(): lax.psum_scatter(jnp.dot(hidden, down_weight, preferred_element_type=jnp....]
    all_gather x4 -> x0, blocking collectives: 50.3 us -> none  [the longest x1 31.4 us: per_device(): all_rows = lax.all_gather(second, 'kv', axis=0, tiled=True)]
    pallas_call x0 -> x1, Pallas kernels: none -> 38.8 us  [per_device(): pl.pallas_call(functools.partial(layer_kernel, nkv, ntp), out_shape=(shap...]
    dot_general x10 -> x0, matrix products: 13.3 us -> none  [the longest x1 3.35 us: per_device(): jnp.einsum('bhed,bhd->bhe', memory_new, query_f, precision=lax.Precision....]
    psum x1 -> x0, blocking collectives: 5.67 us -> none  [per_device(): square_sum = lax.psum(square_sum, 'tp')]
    unnamed x22 -> x10, local copies, waits for them, and re-layouts: 2.06 us -> 7.47 us
    convert_element_type x2 -> x0, other arithmetic: 2.51 us -> none  [the longest x1 1.46 us: per_device(): layer_out = (second.astype(jnp.float32) + summed).astype(jnp.bfloat16)]
  transfers between devices with their start and end apart: 2 -> 0, of which waited for: 2 -> 0; matrix products, arithmetic and copies ran while one was open for 0% -> 0% of each run, Pallas kernels for 0% -> 0%
where the time goes in v1:
time: 51.6 us; the launch traced here: 51.3 us
  Pallas kernels  38.8 us (75%)
  local copies, waits for them, and re-layouts  7.47 us (14%)
  other arithmetic  4.36 us (8%)
  between operations  0.64 us (1%)
    pallas_call x1, Pallas kernels, per_device(): pl.pallas_call(functools.partial(layer_kernel, nkv, ntp), out_shape=(shap...  38.8 us
    unnamed x10, local copies, waits for them, and re-layouts  7.47 us
    add x1, other arithmetic, per_device(): keep[..., None, None] * memory + av[..., :, None] * keys[..., None, :]  4.36 us

profile of v1, /device:TPU:0, one launch (start us, length us, event | category | flops | bytes accessed | tf_op | source)
XLA Modules:
  0.0 51.3 jit_solution(9877268528371139452)
XLA Ops:
  0.6 1.4 %copy.21.stab = f32[32,2]{1,0:T(8,128)} copy(f32[32,2]{0,1:T(2,128)} %param.20) | data formatting | bytes 512 | tf_op args[3]
  2.0 1.8 %copy.22.wig = bf16[2048,8]{1,0:T(8,128)(2,1)} copy(bf16[2048,8]{0,1:T(8,128)(2,1)} %param.26) | data formatting | bytes 65536 | tf_op args[9]
  3.8 1.8 %copy.23.wfg = bf16[2048,8]{1,0:T(8,128)(2,1)} copy(bf16[2048,8]{0,1:T(8,128)(2,1)} %param.27) | data formatting | bytes 65536 | tf_op args[10]
  5.5 38.8 %layer.1 = (bf16[32,512]{1,0:T(8,128)(2,1)}, f32[32,2,128]{2,1,0:T(2,128)}, f32[32,2]{1,0:T(8,128)}, f32[32,2]{1,0:T(8,128)}, f32[32,2,128]{2,1,0:T(2,128)}, /*index=5*/f32[32,2,128]{2,1,0:T(2,128)}) custom-call(bf16[32,512]{1,0:T(8,128)(2,1)} %tok.1, f32[32,2,128,128]{3,2,1,0:T(8,128)} %mem_h.1, f32[32,2,128]{2,1,0:T(2,128)} %nrm.1, f32[32,2]{1,0:T(8,128)} %copy.21.stab, ...), custom_call_target="tpu_custom_call" | custom-call | tf_op jit(solution)/shard_map/layer/pallas_call | solution.py:387
  44.3 1.4 %copy.24 = f32[32,2]{0,1:T(2,128)} copy(f32[32,2]{1,0:T(8,128)} %get-tuple-element.19) | data formatting | bytes 512
  45.7 0.0 copy-start.1
  45.7 0.0 copy-start
  45.7 4.4 %multiply_add_fusion = f32[32,2,128,128]{3,2,1,0:T(8,128)} fusion(f32[32,2,128,128]{3,2,1,0:T(8,128)} %mem_h.1, f32[32,2,128]{2,1,0:T(2,128)} %get-tuple-element.13, f32[32,2,128]{2,1,0:T(2,128)} %get-tuple-element.12, f32[32,2]{1,0:T(8,128)} %get-tuple-element.11), kind=kLoop, calls=%fused_computation | loop fusion | flops 3145728 | bytes 8454400 | tf_op jit(solution)/shard_map/add | solution.py:465
  50.0 0.0 copy-done.1
  50.0 0.6 %copy.27 = bf16[32,512]{1,0:T(8,128)(2,1)} copy(bf16[32,512]{1,0:T(8,128)(2,1)S(1)} %copy-done.1) | data formatting | bytes 65536
  50.6 0.0 copy-done
  50.6 0.6 %copy.28 = f32[32,2,128]{2,1,0:T(2,128)} copy(f32[32,2,128]{2,1,0:T(2,128)S(1)} %copy-done) | data formatting | bytes 65536
Async XLA Ops:
  45.7 4.4 %copy-start.1 = (bf16[32,512]{1,0:T(8,128)(2,1)S(1)}, bf16[32,512]{1,0:T(8,128)(2,1)}, u32[]{:S(2)}) copy-start(bf16[32,512]{1,0:T(8,128)(2,1)} %get-tuple-element.24) | copy-start | bytes 98308
  45.7 5.0 %copy-start = (f32[32,2,128]{2,1,0:T(2,128)S(1)}, f32[32,2,128]{2,1,0:T(2,128)}, u32[]{:S(2)}) copy-start(f32[32,2,128]{2,1,0:T(2,128)} %get-tuple-element.26) | copy-start | bytes 98308

commit v2 on v1

--- a/solution.py
+++ b/solution.py
@@ -18,33 +18,44 @@
     return jnp.dot(a, b, preferred_element_type=F32)
 
 
+def dot_nt(a, b):
+    return lax.dot_general(a, b, (((1,), (1,)), ((), ())), preferred_element_type=F32)
+
+
 def layer_kernel(
     nkv,
     ntp,
-    tok,
+    tok_h,
     mem_h,
-    nrm,
-    stab,
-    ngain,
+    nrm_h,
+    stab_h,
+    ngain_h,
     wq_h,
     wk_h,
     wv_h,
     wo_h,
-    wig,
-    wfg,
-    fbias,
-    mgain,
+    wig_h,
+    wfg_h,
+    fbias_h,
+    mgain_h,
     wp_h,
-    fgain,
+    fgain_h,
     wu_h,
     wd_h,
     out,
     nrm_new,
     stab_new,
-    keep_out,
-    av_out,
-    key_out,
     mem,
+    nrm,
+    stab,
+    ngain,
+    wig,
+    wfg,
+    fbias,
+    mgain,
+    fgain,
+    mem_b,
+    rowed,
     wqkv,
     wp,
     wu,
@@ -64,6 +75,7 @@
     part_s,
     part_r,
     down_own,
+    s_sem,
     w_sem,
     p_sem,
     f_sem,
@@ -85,7 +97,8 @@
     r_send,
     r_recv,
 ):
-    rows, width = tok.shape
+    rows, width = tok_h.shape
+    tok = tokg.at[0]
     heads, dk = nrm.shape[1], nrm.shape[2]
     cols = heads * dk
     features = width * ntp
@@ -103,6 +116,24 @@
     def kv_at(dz, dx):
         return ((z + dz + nz) % nz) * 2 + (x + dx + 2) % 2
 
+    small = [
+        pltpu.make_async_copy(s, t, s_sem.at[i])
+        for i, (s, t) in enumerate(
+            (
+                (tok_h, tok),
+                (ngain_h, ngain),
+                (wig_h, wig),
+                (wfg_h, wfg),
+                (fbias_h, fbias),
+                (stab_h, stab),
+                (nrm_h, nrm),
+                (mgain_h, mgain),
+                (fgain_h, fgain),
+            )
+        )
+    ]
+    for cp in small:
+        cp.start()
     wcopies = []
     for d, (dy, dc) in enumerate(tps):
         src = tp_at(-dy, -dc)
@@ -160,36 +191,47 @@
         sends.append(cp)
         return cp
 
+    small[0].wait()
     tok_in = [None]
     for d, (dy, dc) in enumerate(tps):
         if d:
             tok_in.append(
                 send(tok, tokg.at[d], tp_send.at[d], tp_recv.at[d], {"tp": tp_at(dy, dc)})
             )
+    for cp in small[1:]:
+        cp.wait()
     acc = jnp.zeros((rows, 4 * cols), F32)
-    in_acc = jnp.zeros((rows, wig.shape[1]), F32)
-    fg_acc = jnp.zeros((rows, wig.shape[1]), F32)
+    in_acc = jnp.zeros((rows, wig.shape[0]), F32)
+    fg_acc = jnp.zeros((rows, wig.shape[0]), F32)
     square = jnp.zeros((rows, 1), F32)
     for d, (dy, dc) in enumerate(tps):
         src = tp_at(-dy, -dc)
         at = pl.ds(pl.multiple_of(src * width, width), width)
         if d:
             tok_in[d].wait_recv()
-        block = (tokg[d] if d else tok[...]).astype(F32)
+        block = tokg[d].astype(F32)
         square += jnp.sum(block * block, axis=1, keepdims=True)
         gained = (block * ngain[:, at]).astype(BF16)
         for cp in wcopies[d]:
             cp.wait()
         acc += dot(gained, wqkv[d])
-        in_acc += dot(gained, wig[at, :])
-        fg_acc += dot(gained, wfg[at, :])
+        in_acc += dot_nt(gained, wig[:, at])
+        fg_acc += dot_nt(gained, wfg[:, at])
+        if d == 0:
+            mcopy.wait()
+            for h in range(heads):
+                for b in range(rows):
+                    mem_b[h, b] = mem[b, h].astype(BF16)
     scale = lax.rsqrt(square / features + EPS)
     acc = acc * scale
     lane = lax.broadcasted_iota(jnp.int32, in_acc.shape, 1)
     in_acc = in_acc * scale
     fg_acc = jax.nn.log_sigmoid(fg_acc * scale + fbias[...])
 
-    mcopy.wait()
+    diagonal = lax.broadcasted_iota(jnp.int32, (rows, rows), 0) == lax.broadcasted_iota(
+        jnp.int32, (rows, rows), 1
+    )
+    admitted = []
     pick = lax.broadcasted_iota(jnp.int32, (GROUP, dk), 0)
     for h in range(heads):
         mine = lane == me_tp * heads + h
@@ -200,25 +242,27 @@
         )
         query_f, values_f, gate_f = query.astype(F32), values.astype(F32), gate.astype(F32)
         keys_f = keys.astype(F32) * dk**-0.5
-        carried = forget_log + stab[:, h : h + 1]
+        before = jnp.sum(
+            jnp.where(diagonal, jnp.broadcast_to(stab[h : h + 1, :], (rows, rows)), 0.0),
+            axis=1,
+            keepdims=True,
+        )
+        carried = forget_log + before
         newest = jnp.maximum(carried, input_log)
         keep = jnp.exp(carried - newest)
         admit = jnp.exp(input_log - newest)
         norm_h = keep * nrm[:, h, :] + admit * keys_f
         nrm_new[:, h, :] = norm_h
-        stab_new[:, h : h + 1] = newest
-        keep_out[:, h : h + 1] = keep
-        av_out[:, h, :] = admit * values_f
-        key_out[:, h, :] = keys_f
+        stab_new[h : h + 1, :] = jnp.sum(
+            jnp.where(diagonal, jnp.broadcast_to(newest, (rows, rows)), 0.0), axis=0, keepdims=True
+        )
+        rowed[h, 0] = jnp.broadcast_to(keep, (rows, dk))
+        rowed[h, 1] = keys_f
+        admitted.append(admit * values_f)
         read = []
         for g in range(rows // GROUP):
-            m = mem[g * GROUP : (g + 1) * GROUP, h].reshape(GROUP * dk, dk).astype(BF16)
-            r = lax.dot_general(
-                query[g * GROUP : (g + 1) * GROUP],
-                m,
-                (((1,), (1,)), ((), ())),
-                preferred_element_type=F32,
-            )
+            m = mem_b[h, g * GROUP : (g + 1) * GROUP].reshape(GROUP * dk, dk)
+            r = dot_nt(query[g * GROUP : (g + 1) * GROUP], m)
             total = jnp.zeros((GROUP, dk), F32)
             for i in range(GROUP):
                 total = jnp.where(pick == i, r[:, i * dk : (i + 1) * dk], total)
@@ -238,6 +282,15 @@
             mix_in.append(
                 send(mixg.at[0], mixg.at[d], mx_send.at[d], mx_recv.at[d], {"tp": tp_at(dy, dc)})
             )
+    for h in range(heads):
+        tall = jnp.transpose(
+            jnp.concatenate([admitted[h], jnp.zeros((dk - rows, dk), F32)], axis=0)
+        )
+        for b in range(rows):
+            mem[b, h] = rowed[h, 0, b : b + 1, :] * mem[b, h] + (
+                tall[:, b : b + 1] * rowed[h, 1, b : b + 1, :]
+            )
+
     second = tok[...].astype(F32)
     for d in range(ntp):
         if d:
@@ -350,6 +403,16 @@
     out[...] = result.astype(BF16)
     for cp in sends:
         cp.wait_send()
+
+
+def put_kernel(*refs):
+    sem = refs[-1]
+    n = (len(refs) - 1) // 2
+    copies = [pltpu.make_async_copy(refs[i], refs[n + i], sem.at[i]) for i in range(n)]
+    for cp in reversed(copies):
+        cp.start()
+    for cp in copies:
+        cp.wait()
 
 
 def per_device(
@@ -382,25 +445,31 @@
     vmem = pl.BlockSpec(memory_space=pltpu.VMEM)
     hbm = pl.BlockSpec(memory_space=pl.ANY)
     dma = pltpu.SemaphoreType.DMA
+    far = functools.partial(pltpu.with_memory_space_constraint, memory_space=pltpu.HBM)
     chunk = (nz, 2 * rows, half)
     blocks = (nz, 2, rows, width)
-    out, nrm_new, stab_new, keep, av, keys = pl.pallas_call(
+    whole = (
+        ((rows, width), BF16),
+        ((rows, heads, dk), F32),
+        ((heads, rows), F32),
+        (memory.shape, F32),
+    )
+    made = pl.pallas_call(
         functools.partial(layer_kernel, nkv, ntp),
-        out_shape=(
-            shape((rows, width), BF16),
-            shape((rows, heads, dk), F32),
-            shape((rows, heads), F32),
-            shape((rows, heads), F32),
-            shape((rows, heads, dk), F32),
-            shape((rows, heads, dk), F32),
-        ),
-        in_specs=[
-            vmem, hbm, vmem, vmem, vmem, hbm, hbm, hbm, hbm, vmem, vmem, vmem, vmem, hbm, vmem,
-            hbm, hbm,
-        ],
-        out_specs=(vmem,) * 6,
+        out_shape=tuple(pltpu.VMEM(*w) for w in whole),
+        in_specs=[hbm] * 17,
+        out_specs=(vmem,) * 4,
         scratch_shapes=[
-            pltpu.VMEM(memory.shape, F32),
+            pltpu.VMEM(normalizer.shape, F32),
+            pltpu.VMEM((heads, rows), F32),
+            pltpu.VMEM((1, width * ntp), F32),
+            pltpu.VMEM(input_gate_weight.shape[::-1], BF16),
+            pltpu.VMEM(input_gate_weight.shape[::-1], BF16),
+            pltpu.VMEM((1, heads * ntp), F32),
+            pltpu.VMEM((1, cols), F32),
+            pltpu.VMEM((1, width), F32),
+            pltpu.VMEM((heads, rows, dk, dk), BF16),
+            pltpu.VMEM((heads, 2, rows, dk), F32),
             pltpu.VMEM((ntp, width, 4 * cols), BF16),
             pltpu.VMEM((ntp, cols, width), BF16),
             pltpu.VMEM((2, width, half), BF16),
@@ -420,6 +489,7 @@
             pltpu.VMEM(blocks, BF16),
             pltpu.VMEM(blocks, BF16),
             pltpu.VMEM((rows, width), F32),
+            dma((9,)),
             dma((ntp, 4)),
             dma((ntp,)),
             dma((2, 2)),
@@ -441,29 +511,44 @@
             dma((nz, 2)),
             dma((nz, 2)),
         ],
-        compiler_params=pltpu.CompilerParams(collective_id=0, has_side_effects=True),
+        compiler_params=pltpu.CompilerParams(
+            collective_id=0, has_side_effects=True, vmem_limit_bytes=40 * 2**20
+        ),
         name="layer",
     )(
-        tokens,
-        memory,
-        normalizer,
-        stabilizer,
-        norm_gain[None, :],
-        query_weight,
-        key_weight,
-        value_weight,
-        outgate_weight,
-        input_gate_weight,
-        forget_gate_weight,
-        forget_bias[None, :],
-        memory_gain[None, :],
-        proj_weight,
-        ffn_gain[None, :],
-        up_weight,
-        down_weight,
+        *map(
+            far,
+            (
+                tokens,
+                memory,
+                normalizer,
+                stabilizer.T,
+                norm_gain[None, :],
+                query_weight,
+                key_weight,
+                value_weight,
+                outgate_weight,
+                input_gate_weight.T,
+                forget_gate_weight.T,
+                forget_bias[None, :],
+                memory_gain[None, :],
+                proj_weight,
+                ffn_gain[None, :],
+                up_weight,
+                down_weight,
+            ),
+        )
     )
-    memory_new = keep[..., None, None] * memory + av[..., :, None] * keys[..., None, :]
-    return (out, memory_new, nrm_new, stab_new)
+    out, nrm_new, stab_new, memory_new = pl.pallas_call(
+        put_kernel,
+        out_shape=tuple(shape(*w) for w in whole),
+        in_specs=[vmem] * 4,
+        out_specs=(hbm,) * 4,
+        scratch_shapes=[dma((4,))],
+        compiler_params=pltpu.CompilerParams(vmem_limit_bytes=2**20),
+        name="put",
+    )(*made)
+    return (out, memory_new, nrm_new, stab_new.T)
 
 
 def solution(mesh):

time: 51.6 us -> 39.6 us (0.77)
  local copies, waits for them, and re-layouts: 7.47 us -> 0 us
  other arithmetic: 4.36 us -> 0 us
    unnamed x10 -> x0, local copies, waits for them, and re-layouts: 7.47 us -> none
    add x1 -> x0, other arithmetic: 4.36 us -> none  [per_device(): keep[..., None, None] * memory + av[..., :, None] * keys[..., None, :]]
    pallas_call x1 -> x2, Pallas kernels: 38.8 us -> 38.8 us  [the longest x1 36.7 us: per_device(): pl.pallas_call(functools.partial(layer_kernel, nkv, ntp), out_shape=tuple...]
where the time goes in v2:
time: 39.6 us; the launch traced here: 39.4 us
  Pallas kernels  38.8 us (98%)
  between operations  0.65 us (2%)
    pallas_call x1, Pallas kernels, per_device(): pl.pallas_call(functools.partial(layer_kernel, nkv, ntp), out_shape=tuple...  36.7 us
    pallas_call x1, Pallas kernels, per_device(): pl.pallas_call(put_kernel, out_shape=tuple((shape(*w) for w in whole)), i...  2.05 us

profile of v2, /device:TPU:0, one launch (start us, length us, event | category | flops | bytes accessed | tf_op | source)
XLA Modules:
  0.0 39.4 jit_solution(1943643914704285610)
XLA Ops:
  0.6 36.7 %layer.1 = (bf16[32,512]{1,0:T(8,128)(2,1)S(1)}, f32[32,2,128]{2,1,0:T(2,128)S(1)}, f32[2,32]{1,0:T(2,128)S(1)}, f32[32,2,128,128]{3,2,1,0:T(8,128)S(1)}) custom-call(bf16[32,512]{1,0:T(8,128)(2,1)} %tok_h.1, f32[32,2,128,128]{3,2,1,0:T(8,128)} %mem_h.1, f32[32,2,128]{2,1,0:T(2,128)} %nrm_h.1, f32[2,32]{1,0:T(2,128)} %bitcast.12, f32[1,2048]{1,0:T(1,128)} %bitcast.10, ...), custom_call_target="tpu_custom_call" | custom-call | tf_op jit(solution)/shard_map/layer/pallas_call | solution.py:457
  37.4 2.1 %put.1 = (bf16[32,512]{1,0:T(8,128)(2,1)}, f32[32,2,128]{2,1,0:T(2,128)}, f32[2,32]{1,0:T(2,128)}, f32[32,2,128,128]{3,2,1,0:T(8,128)}) custom-call(bf16[32,512]{1,0:T(8,128)(2,1)S(1)} %get-tuple-element.12.refs_0_, f32[32,2,128]{2,1,0:T(2,128)S(1)} %get-tuple-element.13.refs_1_, f32[2,32]{1,0:T(2,128)S(1)} %get-tuple-element.14.refs_2_, ...), custom_call_target="tpu_custom_call" | custom-call | tf_op jit(solution)/shard_map/put/pallas_call | solution.py:542
